TPU v7x, 1024 devices: a whole 4x4x32 slice. The times are simulated.
1024 devices in a mesh: kv: 128 (over z, y), tp: 8 (over x, core).
Axes of the slice: x: 4, y: 4, z: 32, core: 2. Of those that a mesh axis runs over, the one named last changes fastest.
Arguments:
- proposals: bfloat16 [256, 4, 4096], P('kv', None, 'tp'), may hold values from -6 to 6
- input_norm_gain: float32 [4096], replicated, may hold values from 0.1 to 1.9
- query_matrix: bfloat16 [4096, 2048], P(None, 'tp'), may hold values from -0.09375 to 0.09375
- forget_gate_matrix: bfloat16 [4096, 2048], P(None, 'tp'), may hold values from -0.09375 to 0.09375
- value_matrix: bfloat16 [4096, 2048], P(None, 'tp'), may hold values from -0.09375 to 0.09375
- forget_floor_channel: float32 [2048], P('tp'), may hold values from 0.02 to 0.95
- proposal_extra_decay: float32 [256, 4, 16], P('kv', None, 'tp'), may hold values from -0.7 to 0
- prior_proposal_states: float32 [256, 4, 2048, 128], P('kv', None, 'tp'), may hold values from -4 to 4
- accepted: int32 [256], P('kv'), may hold values from 1 to 4
- output_matrix: bfloat16 [2048, 4096], P('tp', 'kv'), may hold values from -0.02734375 to 0.02734375
Outputs:
- mixer_output: bfloat16 [256, 4, 4096], P('tp', None, 'kv')
- next_states: float32 [256, 4, 2048, 128], P('kv', None, 'tp')
All inputs are finite; a program needn't handle non-finite values.
Results may differ from a plain program's by a relative error of at most 0.012.
Values may be sent and summed in bfloat16 or wider, within the bound.
No kernel may reach another device: no remote copies, remote signals or barrier semaphores. Data moves between devices by JAX's collectives and lax.ppermute only.
A program may use at most 32 MiB of HBM per device.

v0:
```python
import jax
import jax.numpy as jnp
from jax import lax
from jax.sharding import Mesh
from jax.sharding import PartitionSpec as P

KV = ("kv_0", "kv_1")


def joined_along(pieces, dim):
    shape = list(pieces.shape[1:])
    shape[dim] *= pieces.shape[0]
    return jnp.moveaxis(pieces, 0, dim).reshape(shape)


def copy_for_each(shard, axis):
    devices = lax.axis_size(axis)
    return lax.all_to_all(
        jnp.broadcast_to(shard[None], (devices, *shard.shape)), axis, 0, 0, tiled=True
    )


def gather_directly(shard, axis, dim):
    return joined_along(copy_for_each(shard, axis), dim)


def whole_of(shard, axes, dim):
    if not axes:
        return shard
    nearer = lax.all_gather(shard, axes[-1], axis=dim, tiled=True)
    return whole_of(nearer, axes[:-1], dim)


def split_up(shard, dim, devices):
    before, after = (shard.shape[:dim], shard.shape[dim + 1 :])
    return jnp.moveaxis(shard.reshape(*before, devices, -1, *after), dim, 0)


def summed_on_arrival(shard, axis, dim):
    devices = lax.axis_size(axis)
    pieces = lax.all_to_all(split_up(shard, dim, devices), axis, 0, 0, tiled=True)
    return jnp.sum(pieces, axis=0)


def per_device(
    proposals,
    input_norm_gain,
    query_matrix,
    forget_gate_matrix,
    value_matrix,
    forget_floor_channel,
    proposal_extra_decay,
    prior_proposal_states,
    accepted,
    output_matrix,
):
    seq_count, prop_count, feature_block = proposals.shape
    row_count = seq_count * prop_count
    whole = gather_directly(proposals, "tp", 2)
    flat_rows = whole.reshape(row_count, whole.shape[2]).astype(jnp.float32)
    row_scale = lax.rsqrt(jnp.mean(flat_rows * flat_rows, axis=1) + 1e-06)[:, None]
    scaled = (flat_rows * input_norm_gain).astype(jnp.bfloat16)

    def project(weight):
        return (jnp.dot(scaled, weight, preferred_element_type=jnp.float32) * row_scale).astype(
            jnp.bfloat16
        )

    query_pre = project(query_matrix)
    forget_pre = project(forget_gate_matrix)
    value_pre = project(value_matrix)
    local_width = query_matrix.shape[1]
    head_dim = prior_proposal_states.shape[3]
    local_heads = local_width // head_dim
    head_shape = (seq_count, prop_count, local_heads, head_dim)
    query_act = jax.nn.silu(query_pre.astype(jnp.float32)).reshape(head_shape)
    lower_part = forget_floor_channel.reshape(local_heads, head_dim)
    forget_gate = lower_part + (1.0 - lower_part) * jax.nn.sigmoid(
        forget_pre.astype(jnp.float32).reshape(head_shape)
    )
    forget_gate_logs = jnp.log(forget_gate) + proposal_extra_decay[:, :, :, None]
    key_part = 1.0 - forget_gate
    values = value_pre.astype(jnp.float32).reshape(head_shape)
    picked = jnp.take_along_axis(
        prior_proposal_states, (accepted - 1)[:, None, None, None], axis=1
    )[:, 0]
    carried = picked.reshape(seq_count, local_heads, head_dim, head_dim)
    snapshots = []
    outputs = []
    for position in range(prop_count):
        carried = (
            jnp.exp(forget_gate_logs[:, position])[:, :, None, :] * carried
            + values[:, position][:, :, :, None] * key_part[:, position][:, :, None, :]
        )
        outputs.append(jnp.einsum("shvk,shk->shv", carried, query_act[:, position]))
        snapshots.append(carried.reshape(seq_count, local_width, head_dim))
    mixed_rows = jnp.stack(outputs, axis=1).reshape(row_count, local_width)
    gated_rows = mixed_rows.astype(jnp.bfloat16)
    terms = jnp.dot(whole_of(gated_rows, KV, 0), output_matrix, preferred_element_type=jnp.float32)
    result = summed_on_arrival(terms, "tp", 0)
    out_rows = result.shape[0]
    mixer_output = result.astype(jnp.bfloat16).reshape(
        out_rows // prop_count, prop_count, result.shape[1]
    )
    return (mixer_output, jnp.stack(snapshots, axis=1))


def solution(mesh):
    torus = Mesh(mesh.devices.reshape(32, 4, mesh.shape["tp"]), ("kv_0", "kv_1", "tp"))
    placed = (
        P(KV, None, "tp"),
        P(),
        P(None, "tp"),
        P(None, "tp"),
        P(None, "tp"),
        P("tp"),
        P(KV, None, "tp"),
        P(KV, None, "tp", None),
        P(KV),
        P("tp", KV),
    )
    return jax.shard_map(
        per_device,
        mesh=torus,
        in_specs=placed,
        out_specs=(P("tp", None, KV), P(KV, None, "tp", None)),
        check_vma=False,
    )
```

profile of v0, /device:TPU:1, one launch (start us, length us, event | category | flops | bytes accessed | tf_op | source)
XLA Modules:
  0.0 113.6 jit_solution(5515963125483334065)
XLA Ops:
  0.6 1.5 %broadcast_in_dim.14 = bf16[8,2,4,512]{3,2,1,0:T(4,128)(2,1)} broadcast(bf16[2,4,512]{2,1,0:T(4,128)(2,1)} %param.10), dimensions={1,2,3} | broadcast | bytes 73728 | tf_op jit(solution)/shard_map/broadcast_in_dim | solution.py:19
  2.1 17.4 %all-to-all-start = ((bf16[8,2,4,512]{3,2,1,0:T(4,128)(2,1)}), bf16[8,2,4,512]{3,2,1,0:T(4,128)(2,1)S(1)}, u32[]{:S(2)}, u32[]{:S(2)}) async-start(bf16[8,2,4,512]{3,2,1,0:T(4,128)(2,1)} %broadcast_in_dim.14), calls=%async_computation | async-start | bytes 131072 | tf_op jit(solution)/shard_map/all_to_all | solution.py:18
  19.5 0.7 compare_and_fusion
  20.2 0.7 fusion.45
  20.8 0.1 copy.24
  20.9 0.7 broadcast_subtract_fusion
  21.6 0.8 copy.23
  22.4 0.2 or_reduce_fusion
  22.6 1.8 %gather_fusion = f32[2,256,128]{2,1,0:T(8,128)S(1)} fusion(f32[2,4,256,128]{3,2,1,0:T(8,128)} %param.17, s32[2]{0:T(128)S(1)} %or_reduce_fusion), kind=kCustom, calls=%fused_computation | custom fusion | bytes 524304 | tf_op jit(solution)/shard_map/jit(take_along_axis)/gather | solution.py:84
  24.4 0.1 fusion.21
  24.5 0.1 rsqrt.11
  24.6 0.1 copy.22
  24.7 0.1 copy.38
  24.8 0.7 multiply_convert_fusion
  25.6 0.4 divide_multiply_fusion
  26.0 2.1 %fusion.7 = f32[8,256]{1,0:T(8,128)S(1)} fusion(bf16[8,4096]{1,0:T(8,128)(2,1)S(1)} %multiply_convert_fusion, bf16[4096,256]{1,0:T(8,128)(2,1)} %param.14, f32[8]{0:T(128)S(1)} %rsqrt.11), kind=kOutput, calls=%fused_computation.12 | convolution fusion | flops 16783360 | bytes 2170912 | tf_op jit(solution)/shard_map/dot_general | solution.py:65
  28.1 0.1 copy-done.1
  28.2 0.4 fusion.5
  28.8 0.2 fusion.46
  29.0 0.3 fusion.19
  29.3 0.4 fusion.20
  29.7 0.5 fusion.15
  30.2 9.1 %all_gather.6 = bf16[32,256]{1,0:T(8,128)(2,1)S(1)} all-gather(bf16[8,256]{1,0:T(8,128)(2,1)S(1)} %bitcast.178), channel_id=1, replica_groups=mesh['kv_0'=32,'kv_1'=4,'tp'=8] {'kv_1'}, dimensions={0}, use_global_device_ids=true | all-gather | bytes 20480 | tf_op jit(solution)/shard_map/all_gather | solution.py:30
  39.4 46.2 %all_gather.7 = bf16[1024,256]{1,0:T(8,128)(2,1)S(1)} all-gather(bf16[32,256]{1,0:T(8,128)(2,1)S(1)} %all_gather.6), channel_id=1, replica_groups=mesh['kv_0'=32,'kv_1'=4,'tp'=8] {'kv_0'}, dimensions={0}, use_global_device_ids=true | all-gather | bytes 540672 | tf_op jit(solution)/shard_map/all_gather | solution.py:30
  85.6 0.2 convolution_bitcast_fusion
  85.8 0.7 copy.50
  86.5 21.1 %all-to-all-start.1 = ((f32[8,128,32]{1,2,0:T(8,128)}), f32[8,128,32]{1,2,0:T(8,128)S(1)}, u32[]{:S(2)}, u32[]{:S(2)}) async-start(f32[8,128,32]{1,2,0:T(8,128)} %bitcast.153), calls=%async_computation.1 | async-start | bytes 262144 | tf_op jit(solution)/shard_map/all_to_all | solution.py:41
  107.8 0.3 fusion.11
  108.2 0.2 fusion.10
  108.4 1.0 pad_maximum_fusion
  109.4 3.5 %all-to-all-done.1 = f32[8,128,32]{1,2,0:T(8,128)S(1)} async-done(((f32[8,128,32]{1,2,0:T(8,128)}), f32[8,128,32]{1,2,0:T(8,128)S(1)}, u32[]{:S(2)}, u32[]{:S(2)}) %all-to-all-start.1) | async-done | bytes 131104 | tf_op jit(solution)/shard_map/all_to_all | solution.py:41
  112.9 0.7 copy.27
  (36 shorter events, 0.4 us)
Async XLA Ops:
  0.6 24.9 %copy-start = (bf16[4096,256]{1,0:T(8,128)(2,1)S(1)}, bf16[4096,256]{1,0:T(8,128)(2,1)}, u32[]{:S(2)}) copy-start(bf16[4096,256]{1,0:T(8,128)(2,1)} %param.12) | copy-start | bytes 6291460
  2.1 22.2 %all-to-all-start = ((bf16[8,2,4,512]{3,2,1,0:T(4,128)(2,1)}), bf16[8,2,4,512]{3,2,1,0:T(4,128)(2,1)S(1)}, u32[]{:S(2)}, u32[]{:S(2)}) async-start(bf16[8,2,4,512]{3,2,1,0:T(4,128)(2,1)} %broadcast_in_dim.14), calls=%async_computation | async-start | bytes 131072 | tf_op jit(solution)/shard_map/all_to_all | solution.py:18
  26.0 2.2 %copy-start.1 = (bf16[4096,256]{1,0:T(8,128)(2,1)S(1)}, bf16[4096,256]{1,0:T(8,128)(2,1)}, u32[]{:S(2)}) copy-start(bf16[4096,256]{1,0:T(8,128)(2,1)} %param.13) | copy-start | bytes 6291460
  26.0 2.7 %copy-start.3 = (f32[256]{0:T(256)S(1)}, f32[256]{0:T(256)}, u32[]{:S(2)}) copy-start(f32[256]{0:T(256)} %param.15) | copy-start | bytes 3076
  28.6 57.0 %copy-start.2 = (bf16[256,32]{0,1:T(8,128)(2,1)S(1)}, bf16[256,32]{0,1:T(8,128)(2,1)}, u32[]{:S(2)}) copy-start(bf16[256,32]{0,1:T(8,128)(2,1)} %param.19) | copy-start | bytes 49156
  86.5 26.4 %all-to-all-start.1 = ((f32[8,128,32]{1,2,0:T(8,128)}), f32[8,128,32]{1,2,0:T(8,128)S(1)}, u32[]{:S(2)}, u32[]{:S(2)}) async-start(f32[8,128,32]{1,2,0:T(8,128)} %bitcast.153), calls=%async_computation.1 | async-start | bytes 262144 | tf_op jit(solution)/shard_map/all_to_all | solution.py:41
where the time goes:
time: 114 us
  blocking collectives  55.3 us (49%)
  starting transfers between devices  38.5 us (34%)
  local copies, waits for them, and re-layouts  6.17 us (5%)
  other arithmetic  4.75 us (4%)
  matrix products  4.49 us (4%)
  waiting for transfers between devices  3.48 us (3%)
    all_gather x2, blocking collectives, whole_of(): nearer = lax.all_gather(shard, axes[-1], axis=dim, tiled=True)  55.3 us
    all_to_all x1, starting transfers between devices, summed_on_arrival(): lax.all_to_all(split_up(shard, dim, devices), axis, 0, 0, tiled=True)  21.1 us
    all_to_all x1, starting transfers between devices, copy_for_each(): lax.all_to_all(jnp.broadcast_to(shard[None], (devices, *shard.shape)), ax...  17.4 us
    all_to_all x1, waiting for transfers between devices, summed_on_arrival(): lax.all_to_all(split_up(shard, dim, devices), axis, 0, 0, tiled=True)  3.48 us
    dot_general x3, matrix products, project(): jnp.dot(scaled, weight, preferred_element_type=jnp.float32) * row_scale  2.82 us
  transfers between devices with their start and end apart: 2, of which 1 were waited for; matrix products, arithmetic and copies ran while one was open for 6% of the time, Pallas kernels for 0%

commit v1 on v0

v1 whole, which is shorter than its diff:
```python
import jax
import jax.numpy as jnp
from jax import lax
from jax.experimental import pallas as pl
from jax.experimental.pallas import tpu as pltpu
from jax.sharding import Mesh
from jax.sharding import PartitionSpec as P

KV = ("zh", "zl", "y")
SLAB = ("zl", "y")
BF = jnp.bfloat16
F32 = jnp.float32
VM = pl.BlockSpec(memory_space=pltpu.VMEM)
SM = pl.BlockSpec(memory_space=pltpu.SMEM)
HBM = pl.BlockSpec(memory_space=pltpu.HBM)


def grant(mebibytes):
    return pltpu.CompilerParams(vmem_limit_bytes=mebibytes << 20)


def in_hbm(array):
    return pltpu.with_memory_space_constraint(array, pltpu.HBM)


def spread_kernel(rows_ref, weight_ref, rows_out_ref, weight_out_ref):
    seqs, props, width = rows_ref.shape
    rows = rows_ref[...].reshape(seqs * props, width)
    for copy in range(rows_out_ref.shape[0]):
        rows_out_ref[copy] = rows
    for copy in range(weight_out_ref.shape[0]):
        weight_out_ref[copy] = weight_ref[...]


def front_kernel(
    x_ref, gain_ref, floor_ref, picks_ref, extra_ref, wq_ref, wf_ref, wv_ref, prior_ref,
    out_ref, decay_ref, key_ref, value_ref, picked_ref, held_ref, sems, pick_sems,
):
    blocks, rows, width = x_ref.shape
    seqs, channels, dim = picked_ref.shape
    total = blocks * width
    heads = channels // dim
    props = rows // seqs
    weights = (wq_ref, wf_ref, wv_ref)
    copies = [
        [
            pltpu.make_async_copy(
                weight.at[pl.ds(block * width, width)], held_ref.at[at, block], sems.at[at, block]
            )
            for at, weight in enumerate(weights)
        ]
        for block in range(blocks)
    ]
    for group in copies:
        for copy in group:
            copy.start()
    picks = [
        pltpu.make_async_copy(
            prior_ref.at[seq, picks_ref[seq] - 1], picked_ref.at[seq], pick_sems.at[seq]
        )
        for seq in range(seqs)
    ]
    for copy in picks:
        copy.start()
    head_of = lax.broadcasted_iota(jnp.int32, (rows, channels), 1) // dim
    row_of = lax.broadcasted_iota(jnp.int32, (rows, channels), 0)
    extra = jnp.zeros((rows, channels), F32)
    for seq in range(seqs):
        for head in range(heads):
            for prop in range(props):
                here = (row_of == seq * props + prop) & (head_of == head)
                extra = jnp.where(here, extra_ref[seq, head, prop], extra)
    boost = jnp.exp(extra)
    square = jnp.zeros((rows, width), F32)
    scaled = []
    for block in range(blocks):
        x = x_ref[block].astype(F32)
        square = square + x * x
        scaled.append((x * gain_ref[:, block * width : (block + 1) * width]).astype(BF))
    sums = [jnp.zeros((rows, channels), F32) for _ in weights]
    for block in range(blocks):
        for at in range(len(weights)):
            copies[block][at].wait()
            sums[at] = sums[at] + jnp.dot(
                scaled[block], held_ref[at, block], preferred_element_type=F32
            )
    scale = lax.rsqrt(jnp.sum(square, axis=1, keepdims=True) / total + 1e-06)
    query_pre, forget_pre, value = ((s * scale).astype(BF).astype(F32) for s in sums)
    query = query_pre / (1.0 + jnp.exp(-query_pre))
    lower = floor_ref[...]
    forget = lower + (1.0 - lower) / (1.0 + jnp.exp(-forget_pre))
    key = 1.0 - forget
    decay = forget * boost
    decay_ref[...] = decay
    key_ref[...] = key
    value_ref[...] = value

    step = row_of % props
    carried = decay
    through = query
    mixed = jnp.zeros((rows, channels), F32)
    for lag in range(props):
        product = (key if lag == 0 else pltpu.roll(key, lag, 0)) * through
        weight = jnp.zeros((rows, channels), F32)
        for head in range(heads):
            weight = jnp.where(
                head_of == head,
                jnp.sum(product[:, head * dim : (head + 1) * dim], axis=1, keepdims=True),
                weight,
            )
        late = value if lag == 0 else pltpu.roll(value, lag, 0)
        mixed = mixed + jnp.where(step >= lag, weight * late, 0.0)
        earlier = decay if lag == 0 else pltpu.roll(decay, lag, 0)
        through = through * earlier
        if lag > 0:
            carried = jnp.where(step >= lag, carried * earlier, carried)
    reach = query * carried
    for copy in picks:
        copy.wait()
    seq_of = lax.broadcasted_iota(jnp.int32, (rows, dim), 0) // props
    for head in range(heads):
        span = slice(head * dim, (head + 1) * dim)
        old = jnp.zeros((rows, dim), F32)
        for seq in range(seqs):
            part = lax.dot_general(
                reach[:, span],
                picked_ref[seq, span, :],
                (((1,), (1,)), ((), ())),
                precision=lax.Precision.HIGHEST,
                preferred_element_type=F32,
            )
            old = jnp.where(seq_of == seq, part, old)
        gated = (mixed[:, span] + old).astype(BF)
        for copy in range(out_ref.shape[0]):
            out_ref[copy, :, span] = gated


def states_kernel(picked_ref, decay_ref, key_ref, value_ref, out_ref):
    seqs, props, channels, dim = out_ref.shape
    columns = value_ref[...].T
    for seq in range(seqs):
        for head in range(channels // dim):
            span = slice(head * dim, (head + 1) * dim)
            state = picked_ref[seq, span, :]
            for prop in range(props):
                row = seq * props + prop
                state = (
                    decay_ref[row : row + 1, span] * state
                    + columns[span, row : row + 1] * key_ref[row : row + 1, span]
                )
                out_ref[seq, prop, span, :] = state


def partial_kernel(props, features, rows_ref, weight_ref, out_ref, sums_ref):
    groups = 128 // features
    rows = rows_ref[...]
    count = rows.shape[0] // props
    lane_group = lax.broadcasted_iota(jnp.int32, (count, 128), 1) // features
    for chunk in range(sums_ref.shape[0]):
        sums_ref[chunk] = lax.dot_general(
            rows,
            weight_ref[chunk * 128 : (chunk + 1) * 128, :],
            (((1,), (1,)), ((), ())),
            preferred_element_type=F32,
        )
    for chunk in range(sums_ref.shape[0]):
        strips = [sums_ref[chunk, pl.ds(prop, count, stride=props), :] for prop in range(props)]
        for group in range(groups):
            packed = jnp.zeros((count, 128), F32)
            for prop in range(props):
                shift = (prop - group) % groups * features
                moved = strips[prop] if shift == 0 else pltpu.roll(strips[prop], shift, 1)
                packed = jnp.where(lane_group == prop, moved, packed)
            out_ref[chunk * groups + group] = packed


def per_device(
    proposals,
    input_norm_gain,
    query_matrix,
    forget_gate_matrix,
    value_matrix,
    forget_floor_channel,
    proposal_extra_decay,
    prior_proposal_states,
    accepted,
    output_matrix,
):
    seqs, props, width = proposals.shape
    rows = seqs * props
    channels = query_matrix.shape[1]
    dim = prior_proposal_states.shape[3]
    features = output_matrix.shape[1]
    tp = lax.axis_size("tp")
    planes = lax.axis_size("zh")
    slab = lax.axis_size(SLAB)
    shape = jax.ShapeDtypeStruct

    spread, weights = pl.pallas_call(
        spread_kernel,
        out_shape=(
            pltpu.VMEM((tp, rows, width), BF),
            pltpu.VMEM((slab, features, channels), BF),
        ),
        in_specs=[VM] * 2,
        out_specs=[VM] * 2,
        compiler_params=grant(4),
    )(proposals, output_matrix.T)
    whole = lax.all_to_all(spread, "tp", 0, 0, tiled=True)

    out_weight = lax.all_to_all(weights, SLAB, 0, 0, tiled=True)
    out_weight = out_weight.reshape(slab * features, channels)

    blocks = tp
    front = pl.pallas_call(
        front_kernel,
        out_shape=(shape((planes, rows, channels), BF),)
        + (shape((rows, channels), F32),) * 3
        + (shape((seqs, channels, dim), F32),),
        in_specs=[VM] * 3 + [SM] * 2 + [HBM] * 4,
        out_specs=[VM] * 5,
        scratch_shapes=[
            pltpu.VMEM((3, blocks, width, channels), BF),
            pltpu.SemaphoreType.DMA((3, blocks)),
            pltpu.SemaphoreType.DMA((seqs,)),
        ],
        compiler_params=grant(16),
        cost_estimate=pl.CostEstimate(flops=8 << 20, bytes_accessed=6 << 20, transcendentals=0),
    )
    operands = (
        whole,
        input_norm_gain.reshape(1, -1),
        forget_floor_channel.reshape(1, -1),
        accepted,
        proposal_extra_decay.transpose(0, 2, 1),
        *(in_hbm(m) for m in (query_matrix, forget_gate_matrix, value_matrix)),
        in_hbm(prior_proposal_states),
    )
    gated, decay, key, value, picked = front(*operands)
    crossed = lax.all_to_all(gated, "zh", 0, 0, tiled=True)

    states = pl.pallas_call(
        states_kernel,
        out_shape=shape((seqs, props, channels, dim), F32),
        in_specs=[VM] * 4,
        out_specs=VM,
        compiler_params=grant(8),
        cost_estimate=pl.CostEstimate(flops=8 << 20, bytes_accessed=1 << 20, transcendentals=0),
    )
    next_states = states(picked, decay, key, value)

    partial = pl.pallas_call(
        lambda *refs: partial_kernel(props, features, *refs),
        out_shape=pltpu.VMEM((slab, planes * seqs, 128), F32),
        in_specs=[VM] * 2,
        out_specs=VM,
        compiler_params=grant(8),
        scratch_shapes=[pltpu.VMEM((slab * features // 128, planes * rows, 128), F32)],
        cost_estimate=pl.CostEstimate(flops=1 << 20, bytes_accessed=1 << 18, transcendentals=0),
    )(crossed.reshape(planes * rows, channels), out_weight)

    arrived = lax.all_to_all(
        partial.reshape(slab * tp, seqs, 128), ("zl", "y", "tp"), 0, 0, tiled=True
    )
    result = jnp.sum(arrived.reshape(slab, tp, seqs, 128), axis=1).astype(BF)
    return (result.reshape(slab * seqs, props, features), next_states)


def solution(mesh):
    kv, tp = mesh.shape["kv"], mesh.shape["tp"]
    split = Mesh(mesh.devices.reshape(8, kv // 32, 4, tp), ("zh", "zl", "y", "tp"))
    placed = (
        P(KV, None, "tp"),
        P(),
        P(None, "tp"),
        P(None, "tp"),
        P(None, "tp"),
        P("tp"),
        P(KV, None, "tp"),
        P(KV, None, "tp", None),
        P(KV),
        P("tp", KV),
    )
    return jax.shard_map(
        per_device,
        mesh=split,
        in_specs=placed,
        out_specs=(P("tp", None, KV), P(KV, None, "tp", None)),
        check_vma=False,
    )
```

time: 114 us -> 106 us (0.930)
  starting transfers between devices: 38.5 us -> 8.4 us
  blocking collectives: 55.3 us -> 74.7 us
  Pallas kernels: 0 us -> 7.28 us
  waiting for transfers between devices: 3.48 us -> 9.44 us
  other arithmetic: 4.75 us -> 0.03 us
  matrix products: 4.49 us -> 0 us
  local copies, waits for them, and re-layouts: 6.17 us -> 4.84 us
    all_to_all x0 -> x3, blocking collectives: none -> 74.7 us  [the longest x1 38.9 us: per_device(): crossed = lax.all_to_all(gated, 'zh', 0, 0, tiled=True)]
    all_gather x2 -> x0, blocking collectives: 55.3 us -> none  [whole_of(): nearer = lax.all_gather(shard, axes[-1], axis=dim, tiled=True)]
    all_to_all x2 -> x1, starting transfers between devices: 38.5 us -> 8.4 us  [per_device(): lax.all_to_all(partial.reshape(slab * tp, seqs, 128), ('zl', 'y', 'tp'),...]
    pallas_call x0 -> x4, Pallas kernels: none -> 7.28 us  [the longest x1 4.78 us: per_device(): gated, decay, key, value, picked = front(*operands)]
    all_to_all x2 -> x1, waiting for transfers between devices: 3.48 us -> 9.44 us  [per_device(): lax.all_to_all(partial.reshape(slab * tp, seqs, 128), ('zl', 'y', 'tp'),...]
    dot_general x8 -> x0, matrix products: 4.49 us -> none  [the longest x3 2.82 us: project(): jnp.dot(scaled, weight, preferred_element_type=jnp.float32) * row_scale]
    unnamed x13 -> x12, local copies, waits for them, and re-layouts: 1.01 us -> 4.14 us
    gather x2 -> x0, local copies, waits for them, and re-layouts: 1.89 us -> none  [per_device(): jnp.take_along_axis(prior_proposal_states, (accepted - 1)[:, None, None,...]
  transfers between devices with their start and end apart: 2 -> 1, of which waited for: 1 -> 1; matrix products, arithmetic and copies ran while one was open for 6% -> 0% of each run, Pallas kernels for 0% -> 1%
where the time goes in v1:
time: 106 us; the launch traced here: 105 us
  blocking collectives  74.7 us (70%)
  waiting for transfers between devices  9.44 us (9%)
  starting transfers between devices  8.4 us (8%)
  Pallas kernels  7.28 us (7%)
  local copies, waits for them, and re-layouts  4.84 us (5%)
    all_to_all x1, blocking collectives, per_device(): crossed = lax.all_to_all(gated, 'zh', 0, 0, tiled=True)  38.9 us
    all_to_all x1, blocking collectives, per_device(): whole = lax.all_to_all(spread, 'tp', 0, 0, tiled=True)  21.3 us
    all_to_all x1, blocking collectives, per_device(): out_weight = lax.all_to_all(weights, SLAB, 0, 0, tiled=True)  14.4 us
    all_to_all x1, waiting for transfers between devices, per_device(): lax.all_to_all(partial.reshape(slab * tp, seqs, 128), ('zl', 'y', 'tp'),...  9.44 us
    all_to_all x1, starting transfers between devices, per_device(): lax.all_to_all(partial.reshape(slab * tp, seqs, 128), ('zl', 'y', 'tp'),...  8.4 us
    pallas_call x1, Pallas kernels, per_device(): gated, decay, key, value, picked = front(*operands)  4.78 us
    unnamed x12, local copies, waits for them, and re-layouts  4.14 us
  transfers between devices with their start and end apart: 1, of which 1 were waited for; matrix products, arithmetic and copies ran while one was open for 0% of the time, Pallas kernels for 1%

profile of v1, /device:TPU:1, one launch (start us, length us, event | category | flops | bytes accessed | tf_op | source)
XLA Modules:
  0.0 105.3 jit_solution(11739047467447599549)
XLA Ops:
  0.6 0.0 copy-start.1
  0.6 0.7 copy-done.1
  1.3 0.0 copy-start.2
  1.4 0.7 copy-done.2
  2.1 21.3 %all_to_all.20.x_ref = bf16[8,8,512]{2,1,0:T(8,128)(2,1)S(1)} all-to-all(bf16[8,8,512]{2,1,0:T(8,128)(2,1)S(1)} %get-tuple-element.9), channel_id=1, replica_groups=mesh['zh'=8,'zl'=4,'y'=4,'tp'=8] {'tp'}, dimensions={0} | all-to-all | bytes 131072 | tf_op jit(solution)/shard_map/all_to_all | solution.py:209
  23.4 0.0 copy-start
  23.4 0.7 copy-done
  24.1 0.0 copy-start.3
  24.1 0.7 copy-done.3
  24.8 0.0 copy-start.4
  24.8 0.7 copy-done.4
  25.5 0.0 copy-start.5
  25.5 0.7 copy-done.5
  26.1 4.8 %shard_map.114 = (bf16[8,8,256]{2,1,0:T(8,128)(2,1)S(1)}, f32[8,256]{1,0:T(8,128)S(1)}, f32[8,256]{1,0:T(8,128)S(1)}, f32[8,256]{1,0:T(8,128)S(1)}, f32[2,256,128]{2,1,0:T(8,128)S(1)}) custom-call(bf16[8,8,512]{2,1,0:T(8,128)(2,1)S(1)} %all_to_all.20.x_ref, f32[1,4096]{1,0:T(1,128)S(1)} %bitcast.11, f32[1,256]{1,0:T(1,128)S(1)} %bitcast.14, s32[2]{0:T(128)S(1)} %copy-done.5, ...), custom_call_target="tpu_custom_call" | custom-call | flops 8388608 | bytes 6291456 | tf_op jit(solution)/shard_map/pallas_call | solution.py:239
  30.9 38.9 %all_to_all.21 = bf16[8,8,256]{2,1,0:T(8,128)(2,1)S(1)} all-to-all(bf16[8,8,256]{2,1,0:T(8,128)(2,1)S(1)} %get-tuple-element.10), channel_id=1, replica_groups=mesh['zh'=8,'zl'=4,'y'=4,'tp'=8] {'zh'}, dimensions={0} | all-to-all | bytes 65536 | tf_op jit(solution)/shard_map/all_to_all | solution.py:240
  69.8 14.4 %all_to_all.22 = bf16[16,32,256]{2,1,0:T(8,128)(2,1)S(1)} all-to-all(bf16[16,32,256]{2,1,0:T(8,128)(2,1)S(1)} %get-tuple-element.11), channel_id=1, replica_groups=mesh['zh'=8,'zl'=4,'y'=4,'tp'=8] {'zl','y'}, dimensions={0} | all-to-all | bytes 524288 | tf_op jit(solution)/shard_map/all_to_all | solution.py:211
  84.3 1.0 shard_map.115
  85.3 8.4 %all-to-all-start.3 = ((f32[128,2,128]{2,1,0:T(2,128)}), f32[128,2,128]{2,1,0:T(2,128)S(1)}, u32[]{:S(2)}, u32[]{:S(2)}) async-start(f32[128,2,128]{2,1,0:T(2,128)} %bitcast.6), calls=%async_computation.3 | async-start | bytes 262144 | tf_op jit(solution)/shard_map/all_to_all | solution.py:262
  93.7 1.5 %shard_map.116 = f32[2,4,256,128]{3,2,1,0:T(8,128)} custom-call(f32[2,256,128]{2,1,0:T(8,128)S(1)} %get-tuple-element.12.picked_ref, f32[8,256]{1,0:T(8,128)S(1)} %get-tuple-element.13.decay_ref, f32[8,256]{1,0:T(8,128)S(1)} %get-tuple-element.14.key_ref, f32[8,256]{1,0:T(8,128)S(1)} %get-tuple-element.15.value_ref), custom_call_target="tpu_custom_call" | custom-call | flops 8388608 | bytes 1048576 | tf_op jit(solution)/shard_map/pallas_call | solution.py:250
  95.2 9.4 %all-to-all-done.3 = f32[128,2,128]{2,1,0:T(2,128)S(1)} async-done(((f32[128,2,128]{2,1,0:T(2,128)}), f32[128,2,128]{2,1,0:T(2,128)S(1)}, u32[]{:S(2)}, u32[]{:S(2)}) %all-to-all-start.3) | async-done | bytes 131104 | tf_op jit(solution)/shard_map/all_to_all | solution.py:262
  104.6 0.7 convert_element_type.8
  (2 shorter events, 0.1 us)
Async XLA Ops:
  0.6 0.7 copy-start.1
  1.3 0.7 copy-start.2
  23.4 0.7 copy-start
  24.1 0.7 copy-start.3
  24.8 0.7 copy-start.4
  25.5 0.7 copy-start.5
  85.3 19.3 %all-to-all-start.3 = ((f32[128,2,128]{2,1,0:T(2,128)}), f32[128,2,128]{2,1,0:T(2,128)S(1)}, u32[]{:S(2)}, u32[]{:S(2)}) async-start(f32[128,2,128]{2,1,0:T(2,128)} %bitcast.6), calls=%async_computation.3 | async-start | bytes 262144 | tf_op jit(solution)/shard_map/all_to_all | solution.py:262

commit v2 on v1

v2 whole, which is shorter than its diff:
```python
import jax
import jax.numpy as jnp
from jax import lax
from jax.experimental import pallas as pl
from jax.experimental.pallas import tpu as pltpu
from jax.sharding import Mesh
from jax.sharding import PartitionSpec as P

KV = ("zh", "zl", "y")
SLAB = ("zl", "y")
BF = jnp.bfloat16
F32 = jnp.float32
VM = pl.BlockSpec(memory_space=pltpu.VMEM)
ZL_FIRST = 1
TP_FIRST = 1
HBM = pl.BlockSpec(memory_space=pltpu.HBM)


def exchange(pieces, axes, order):
    return lax.all_to_all(pieces, axes, 0, 0, tiled=True, axis_index_groups=[list(order)])


def led_by(count, first):
    return [first] + [at for at in range(count) if at != first]


def grant(mebibytes):
    return pltpu.CompilerParams(vmem_limit_bytes=mebibytes << 20)


def in_hbm(array):
    return pltpu.with_memory_space_constraint(array, pltpu.HBM)


def spread_kernel(rows_ref, weight_ref, out_ref, held_ref, kept_ref, sems):
    copies = [
        pltpu.make_async_copy(rows_ref, held_ref, sems.at[0]),
        pltpu.make_async_copy(weight_ref, kept_ref, sems.at[1]),
    ]
    for copy in copies:
        copy.start()
    seqs, props, width = held_ref.shape
    count = seqs * props
    features, channels = kept_ref.shape
    half = features // 2
    copies[0].wait()
    rows = held_ref[...].reshape(count, width)
    copies[1].wait()
    for copy in range(out_ref.shape[0]):
        out_ref[copy, :count] = rows
        out_ref[copy, count:, :channels] = kept_ref[:half]
        out_ref[copy, count:, channels:] = kept_ref[half:]


def contract_last(left, right):
    return lax.dot_general(left, right, (((1,), (1,)), ((), ())), preferred_element_type=F32)


def front_kernel(
    order, picks_from, extra_from, x_ref, gain_from, floor_from, wq_ref, wf_ref, wv_ref, prior_ref,
    out_ref, decay_ref, key_ref, value_ref, picked_ref,
    picks_ref, extra_ref, gain_ref, floor_ref, held_ref, small_sems, sems, pick_sems,
):
    small = [
        pltpu.make_async_copy(source, kept, small_sems.at[at])
        for at, (source, kept) in enumerate(
            (
                (picks_from, picks_ref),
                (gain_from, gain_ref),
                (extra_from, extra_ref),
                (floor_from, floor_ref),
            )
        )
    ]
    for copy in small:
        copy.start()
    seqs, channels, dim = picked_ref.shape
    rows = decay_ref.shape[0]
    blocks, _, width = x_ref.shape
    total = blocks * width
    heads = channels // dim
    props = rows // seqs
    weights = (wq_ref, wf_ref, wv_ref)
    copies = [
        [
            pltpu.make_async_copy(
                weight.at[pl.ds(order[block] * width, width)], held_ref.at[at, block], sems.at[at, block]
            )
            for at, weight in enumerate(weights)
        ]
        for block in range(blocks)
    ]
    for group in copies:
        for copy in group:
            copy.start()
    small[0].wait()
    picks = [
        pltpu.make_async_copy(
            prior_ref.at[seq, picks_ref[seq] - 1], picked_ref.at[seq], pick_sems.at[seq]
        )
        for seq in range(seqs)
    ]
    for copy in picks:
        copy.start()
    for copy in small[1:]:
        copy.wait()
    square = jnp.zeros((rows, width), F32)
    scaled = []
    for block in range(blocks):
        x = x_ref[block, :rows].astype(F32)
        square = square + x * x
        scaled.append((x * gain_ref[:, order[block] * width : (order[block] + 1) * width]).astype(BF))
    head_of = lax.broadcasted_iota(jnp.int32, (rows, channels), 1) // dim
    row_of = lax.broadcasted_iota(jnp.int32, (rows, channels), 0)
    extra = jnp.zeros((rows, channels), F32)
    for seq in range(seqs):
        for head in range(heads):
            for prop in range(props):
                here = (row_of == seq * props + prop) & (head_of == head)
                extra = jnp.where(here, extra_ref[seq, head, prop], extra)
    boost = jnp.exp(extra)
    sums = [jnp.zeros((rows, channels), F32) for _ in weights]
    for block in range(blocks):
        for at in range(len(weights)):
            copies[block][at].wait()
            sums[at] = sums[at] + jnp.dot(
                scaled[block], held_ref[at, block], preferred_element_type=F32
            )
    scale = lax.rsqrt(jnp.sum(square, axis=1, keepdims=True) / total + 1e-06)
    query_pre, forget_pre, value = ((s * scale).astype(BF).astype(F32) for s in sums)
    query = query_pre / (1.0 + jnp.exp(-query_pre))
    lower = floor_ref[...]
    forget = lower + (1.0 - lower) / (1.0 + jnp.exp(-forget_pre))
    key = 1.0 - forget
    decay = forget * boost
    decay_ref[...] = decay
    key_ref[...] = key
    value_ref[...] = value

    step = row_of % props
    carried = decay
    through = query
    mixed = jnp.zeros((rows, channels), F32)
    for lag in range(props):
        product = (key if lag == 0 else pltpu.roll(key, lag, 0)) * through
        weight = jnp.zeros((rows, channels), F32)
        for head in range(heads):
            weight = jnp.where(
                head_of == head,
                jnp.sum(product[:, head * dim : (head + 1) * dim], axis=1, keepdims=True),
                weight,
            )
        late = value if lag == 0 else pltpu.roll(value, lag, 0)
        mixed = mixed + jnp.where(step >= lag, weight * late, 0.0)
        earlier = decay if lag == 0 else pltpu.roll(decay, lag, 0)
        through = through * earlier
        if lag > 0:
            carried = jnp.where(step >= lag, carried * earlier, carried)
    reach = query * carried
    high = reach.astype(BF)
    low = (reach - high.astype(F32)).astype(BF)
    reach = jnp.concatenate([high, low], axis=0)
    for copy in picks:
        copy.wait()
    seq_of = lax.broadcasted_iota(jnp.int32, (rows, dim), 0) // props
    for head in range(heads):
        span = slice(head * dim, (head + 1) * dim)
        old = jnp.zeros((rows, dim), F32)
        for seq in range(seqs):
            state = picked_ref[seq, span, :]
            state_high = state.astype(BF)
            state_low = (state - state_high.astype(F32)).astype(BF)
            part = contract_last(reach[:, span], state_high)
            part = part[:rows] + part[rows:] + contract_last(high[:, span], state_low)
            old = jnp.where(seq_of == seq, part, old)
        gated = (mixed[:, span] + old).astype(BF)
        for copy in range(out_ref.shape[0]):
            out_ref[copy, :, span] = gated


def states_kernel(picked_ref, decay_ref, key_ref, value_ref, out_ref):
    seqs, props, channels, dim = out_ref.shape
    columns = value_ref[...].T
    for seq in range(seqs):
        for head in range(channels // dim):
            span = slice(head * dim, (head + 1) * dim)
            state = picked_ref[seq, span, :]
            for prop in range(props):
                row = seq * props + prop
                state = (
                    decay_ref[row : row + 1, span] * state
                    + columns[span, row : row + 1] * key_ref[row : row + 1, span]
                )
                out_ref[seq, prop, span, :] = state


def repeat_kernel(rows_ref, out_ref):
    for copy in range(out_ref.shape[0]):
        out_ref[copy] = rows_ref[...]


def product_kernel(order, rows, features, rows_ref, weight_ref, out_ref):
    members, blocks, _, channels = rows_ref.shape
    total = jnp.zeros((members * rows, features), F32)
    for block in range(blocks):
        left = jnp.concatenate([rows_ref[order.index(at), block] for at in range(members)], axis=0)
        right = jnp.concatenate(
            [weight_ref[block, rows:, :channels], weight_ref[block, rows:, channels:]], axis=0
        )
        total = total + contract_last(left, right)
    out_ref[...] = total.astype(BF)


def per_device(
    proposals,
    input_norm_gain,
    query_matrix,
    forget_gate_matrix,
    value_matrix,
    forget_floor_channel,
    proposal_extra_decay,
    prior_proposal_states,
    accepted,
    output_matrix,
):
    seqs, props, width = proposals.shape
    rows = seqs * props
    channels = query_matrix.shape[1]
    dim = prior_proposal_states.shape[3]
    features = output_matrix.shape[1]
    tp = lax.axis_size("tp")
    planes = lax.axis_size("zh")
    slab = lax.axis_size(SLAB)
    shape = jax.ShapeDtypeStruct
    tp_order = led_by(tp, TP_FIRST)
    zl_order = led_by(lax.axis_size("zl"), ZL_FIRST)
    side = lax.axis_size("y")
    slab_order = [zl * side + y for zl in zl_order for y in range(side)]

    pieces = pl.pallas_call(
        spread_kernel,
        out_shape=pltpu.VMEM((tp, rows + features * channels // width, width), BF),
        in_specs=[HBM] * 2,
        out_specs=VM,
        scratch_shapes=[
            pltpu.VMEM(proposals.shape, BF),
            pltpu.VMEM((features, channels), BF),
            pltpu.SemaphoreType.DMA((2,)),
        ],
        compiler_params=grant(4),
    )(in_hbm(proposals), in_hbm(output_matrix.T))
    whole = exchange(pieces, "tp", tp_order)

    blocks = tp
    front = pl.pallas_call(
        lambda *refs: front_kernel(tp_order, *refs),
        out_shape=(pltpu.VMEM((tp, rows, channels), BF),)
        + (shape((rows, channels), F32),) * 3
        + (shape((seqs, channels, dim), F32),),
        in_specs=[HBM] * 2 + [VM] + [HBM] * 6,
        out_specs=[VM] * 5,
        scratch_shapes=[
            pltpu.SMEM(accepted.shape, jnp.int32),
            pltpu.SMEM((seqs, channels // dim, props), F32),
            pltpu.VMEM((1, tp * width), F32),
            pltpu.VMEM((1, channels), F32),
            pltpu.VMEM((3, blocks, width, channels), BF),
            pltpu.SemaphoreType.DMA((4,)),
            pltpu.SemaphoreType.DMA((3, blocks)),
            pltpu.SemaphoreType.DMA((seqs,)),
        ],
        compiler_params=grant(16),
        cost_estimate=pl.CostEstimate(flops=8 << 20, bytes_accessed=6 << 20, transcendentals=0),
    )
    operands = (
        in_hbm(accepted),
        in_hbm(proposal_extra_decay.transpose(0, 2, 1)),
        whole,
        in_hbm(input_norm_gain.reshape(1, -1)),
        in_hbm(forget_floor_channel.reshape(1, -1)),
        *(in_hbm(m) for m in (query_matrix, forget_gate_matrix, value_matrix)),
        in_hbm(prior_proposal_states),
    )
    gated, decay, key, value, picked = front(*operands)
    full = exchange(gated, "tp", tp_order)
    swap = [(zh * tp + t, t * tp + zh) for zh in range(planes) for t in range(tp)]
    crossed = lax.ppermute(full, ("zh", "tp"), swap)

    states = pl.pallas_call(
        states_kernel,
        out_shape=shape((seqs, props, channels, dim), F32),
        in_specs=[VM] * 4,
        out_specs=VM,
        compiler_params=grant(8),
        cost_estimate=pl.CostEstimate(flops=8 << 20, bytes_accessed=1 << 20, transcendentals=0),
    )
    next_states = states(picked, decay, key, value)

    repeated = pl.pallas_call(
        repeat_kernel,
        out_shape=pltpu.VMEM((slab, *crossed.shape), BF),
        in_specs=[VM],
        out_specs=VM,
        compiler_params=grant(4),
    )(crossed)
    gathered = exchange(repeated, SLAB, slab_order)
    result = pl.pallas_call(
        lambda *refs: product_kernel(slab_order, rows, features, *refs),
        out_shape=shape((slab * rows, features), BF),
        in_specs=[VM] * 2,
        out_specs=VM,
        compiler_params=grant(8),
    )(gathered, whole)
    return (result.reshape(slab * seqs, props, features), next_states)


def solution(mesh):
    kv, tp = mesh.shape["kv"], mesh.shape["tp"]
    split = Mesh(mesh.devices.reshape(tp, kv // (4 * tp), 4, tp), ("zh", "zl", "y", "tp"))
    placed = (
        P(KV, None, "tp"),
        P(),
        P(None, "tp"),
        P(None, "tp"),
        P(None, "tp"),
        P("tp"),
        P(KV, None, "tp"),
        P(KV, None, "tp", None),
        P(KV),
        P("tp", KV),
    )
    return jax.shard_map(
        per_device,
        mesh=split,
        in_specs=placed,
        out_specs=(P("tp", None, KV), P(KV, None, "tp", None)),
        check_vma=False,
    )
```

time: 106 us -> 77.8 us (0.73)
  the two profiles are of different devices: /device:TPU:1 before, /device:TPU:4 now
where the time goes in v2:
time: 77.8 us; the launch traced here: 77.4 us
  blocking collectives  26.1 us (34%)
  starting transfers between devices  24.3 us (31%)
  waiting for transfers between devices  17 us (22%)
  Pallas kernels  9.34 us (12%)
    all_to_all x2, blocking collectives, exchange(): lax.all_to_all(pieces, axes, 0, 0, tiled=True, axis_index_groups=[list(or...  26.1 us
    ppermute x1, starting transfers between devices, per_device(): crossed = lax.ppermute(full, ('zh', 'tp'), swap)  20.8 us
    all_to_all x1, waiting for transfers between devices, exchange(): lax.all_to_all(pieces, axes, 0, 0, tiled=True, axis_index_groups=[list(or...  11.3 us
    ppermute x1, waiting for transfers between devices, per_device(): crossed = lax.ppermute(full, ('zh', 'tp'), swap)  5.71 us
    pallas_call x1, Pallas kernels, per_device(): gated, decay, key, value, picked = front(*operands)  5.37 us
    all_to_all x1, starting transfers between devices, exchange(): lax.all_to_all(pieces, axes, 0, 0, tiled=True, axis_index_groups=[list(or...  3.47 us
  transfers between devices with their start and end apart: 2, of which 2 were waited for; matrix products, arithmetic and copies ran while one was open for 0% of the time, Pallas kernels for 2%

profile of v2, /device:TPU:4, one launch (start us, length us, event | category | flops | bytes accessed | tf_op | source)
XLA Modules:
  0.0 77.4 jit_solution(3394113121875133524)
XLA Ops:
  0.6 0.8 shard_map.113
  1.4 18.2 %all_to_all.15.refs_2_.refs_1_ = bf16[8,24,512]{2,1,0:T(8,128)(2,1)S(1)} all-to-all(bf16[8,24,512]{2,1,0:T(8,128)(2,1)S(1)} %shard_map.113), channel_id=1, replica_groups={{1,0,2,3,4,5,6,7},{9,8,10,11,12,13,14,15},{17,16,18,19,20,21,22,23},{25..., dimensions={0} | all-to-all | bytes 393216 | tf_op jit(solution)/shard_map/all_to_all | solution.py:20
  19.6 5.4 %shard_map.114 = (bf16[8,8,256]{2,1,0:T(8,128)(2,1)S(1)}, f32[8,256]{1,0:T(8,128)S(1)}, f32[8,256]{1,0:T(8,128)S(1)}, f32[8,256]{1,0:T(8,128)S(1)}, f32[2,256,128]{2,1,0:T(8,128)S(1)}) custom-call(s32[2]{0:T(128)} %refs_0_.1, f32[2,2,4]{2,1,0:T(2,128)} %bitcast.8, bf16[8,24,512]{2,1,0:T(8,128)(2,1)S(1)} %all_to_all.15.refs_2_.refs_1_, f32[1,4096]{1,0:T(1,128)} %bitcast.6, ...), custom_call_target="tpu_custom_call" | custom-call | flops 8388608 | bytes 6291456 | tf_op jit(solution)/shard_map/pallas_call | solution.py:284
  25.0 7.8 %all_to_all.16 = bf16[8,8,256]{2,1,0:T(8,128)(2,1)S(1)} all-to-all(bf16[8,8,256]{2,1,0:T(8,128)(2,1)S(1)} %get-tuple-element.7), channel_id=1, replica_groups={{1,0,2,3,4,5,6,7},{9,8,10,11,12,13,14,15},{17,16,18,19,20,21,22,23},{25..., dimensions={0} | all-to-all | bytes 65536 | tf_op jit(solution)/shard_map/all_to_all | solution.py:20
  32.9 20.8 %collective-permute-start = (bf16[8,8,256]{2,1,0:T(8,128)(2,1)S(1)}, bf16[8,8,256]{2,1,0:T(8,128)(2,1)S(1)}, u32[]{:S(2)}, u32[]{:S(2)}) collective-permute-start(bf16[8,8,256]{2,1,0:T(8,128)(2,1)S(1)} %all_to_all.16), channel_id=1, source_target_pairs={{0,0},{1,128},{2,256},{3,384},{4,512},{5,640},{6,768},{7,896},{128... | collective-permute-start | bytes 98312 | tf_op jit(solution)/shard_map/ppermute | solution.py:287
  53.7 5.7 %collective-permute-done.rows_ref = bf16[8,8,256]{2,1,0:T(8,128)(2,1)S(1)} collective-permute-done((bf16[8,8,256]{2,1,0:T(8,128)(2,1)S(1)}, bf16[8,8,256]{2,1,0:T(8,128)(2,1)S(1)}, u32[]{:S(2)}, u32[]{:S(2)}) %collective-permute-start) | collective-permute-done | bytes 32800 | tf_op jit(solution)/shard_map/ppermute | solution.py:287
  59.4 0.8 %shard_map.115 = bf16[16,8,8,256]{3,2,1,0:T(8,128)(2,1)} custom-call(bf16[8,8,256]{2,1,0:T(8,128)(2,1)S(1)} %collective-permute-done.rows_ref), custom_call_target="tpu_custom_call" | custom-call | tf_op jit(solution)/shard_map/pallas_call | solution.py:299
  60.2 3.5 %all-to-all-start.2 = ((bf16[16,8,8,256]{3,2,1,0:T(8,128)(2,1)}), bf16[16,8,8,256]{3,2,1,0:T(8,128)(2,1)S(1)}, u32[]{:S(2)}, u32[]{:S(2)}) async-start(bf16[16,8,8,256]{3,2,1,0:T(8,128)(2,1)} %shard_map.115), calls=%async_computation.2 | async-start | bytes 1048576 | tf_op jit(solution)/shard_map/all_to_all | solution.py:20
  63.7 1.5 %shard_map.117 = f32[2,4,256,128]{3,2,1,0:T(8,128)} custom-call(f32[2,256,128]{2,1,0:T(8,128)S(1)} %get-tuple-element.8.picked_ref, f32[8,256]{1,0:T(8,128)S(1)} %get-tuple-element.9.decay_ref, f32[8,256]{1,0:T(8,128)S(1)} %get-tuple-element.10.key_ref, f32[8,256]{1,0:T(8,128)S(1)} %get-tuple-element.11.value_ref), custom_call_target="tpu_custom_call" | custom-call | flops 8388608 | bytes 1048576 | tf_op jit(solution)/shard_map/pallas_call | solution.py:297
  65.2 11.3 %all-to-all-done.2.refs_0_ = bf16[16,8,8,256]{3,2,1,0:T(8,128)(2,1)S(1)} async-done(((bf16[16,8,8,256]{3,2,1,0:T(8,128)(2,1)}), bf16[16,8,8,256]{3,2,1,0:T(8,128)(2,1)S(1)}, u32[]{:S(2)}, u32[]{:S(2)}) %all-to-all-start.2) | async-done | bytes 524320 | tf_op jit(solution)/shard_map/all_to_all | solution.py:20
  76.5 0.9 %shard_map.116 = bf16[128,32]{1,0:T(8,128)(2,1)} custom-call(bf16[16,8,8,256]{3,2,1,0:T(8,128)(2,1)S(1)} %all-to-all-done.2.refs_0_, bf16[8,24,512]{2,1,0:T(8,128)(2,1)S(1)} %all_to_all.15.refs_2_.refs_1_), custom_call_target="tpu_custom_call" | custom-call | tf_op jit(solution)/shard_map/pallas_call | solution.py:307
Async XLA Ops:
  32.9 26.5 %collective-permute-start = (bf16[8,8,256]{2,1,0:T(8,128)(2,1)S(1)}, bf16[8,8,256]{2,1,0:T(8,128)(2,1)S(1)}, u32[]{:S(2)}, u32[]{:S(2)}) collective-permute-start(bf16[8,8,256]{2,1,0:T(8,128)(2,1)S(1)} %all_to_all.16), channel_id=1, source_target_pairs={{0,0},{1,128},{2,256},{3,384},{4,512},{5,640},{6,768},{7,896},{128... | collective-permute-start | bytes 98312 | tf_op jit(solution)/shard_map/ppermute | solution.py:287
  60.2 16.3 %all-to-all-start.2 = ((bf16[16,8,8,256]{3,2,1,0:T(8,128)(2,1)}), bf16[16,8,8,256]{3,2,1,0:T(8,128)(2,1)S(1)}, u32[]{:S(2)}, u32[]{:S(2)}) async-start(bf16[16,8,8,256]{3,2,1,0:T(8,128)(2,1)} %shard_map.115), calls=%async_computation.2 | async-start | bytes 1048576 | tf_op jit(solution)/shard_map/all_to_all | solution.py:20

commit v3 on v2

--- a/solution.py
+++ b/solution.py
@@ -13,6 +13,7 @@
 VM = pl.BlockSpec(memory_space=pltpu.VMEM)
 ZL_FIRST = 1
 TP_FIRST = 1
+AHEAD = 5
 HBM = pl.BlockSpec(memory_space=pltpu.HBM)
 
 
@@ -90,9 +91,9 @@
         ]
         for block in range(blocks)
     ]
-    for group in copies:
+    for group in copies[:AHEAD]:
         for copy in group:
-            copy.start()
+            copy.start(priority=1)
     small[0].wait()
     picks = [
         pltpu.make_async_copy(
@@ -123,6 +124,9 @@
     for block in range(blocks):
         for at in range(len(weights)):
             copies[block][at].wait()
+        for copy in copies[block + AHEAD] if block + AHEAD < blocks else ():
+            copy.start(priority=1)
+        for at in range(len(weights)):
             sums[at] = sums[at] + jnp.dot(
                 scaled[block], held_ref[at, block], preferred_element_type=F32
             )
@@ -201,6 +205,7 @@
 
 def product_kernel(order, rows, features, rows_ref, weight_ref, out_ref):
     members, blocks, _, channels = rows_ref.shape
+    half = features // 2
     total = jnp.zeros((members * rows, features), F32)
     for block in range(blocks):
         left = jnp.concatenate([rows_ref[order.index(at), block] for at in range(members)], axis=0)
@@ -208,7 +213,12 @@
             [weight_ref[block, rows:, :channels], weight_ref[block, rows:, channels:]], axis=0
         )
         total = total + contract_last(left, right)
-    out_ref[...] = total.astype(BF)
+    planes = lax.axis_size("zh")
+    far = (lax.axis_index("tp") + planes - lax.axis_index("zh")) % planes == planes // 2
+    half = members * rows // 2
+    out_ref[...] = jnp.where(
+        far, jnp.concatenate([total[half:], total[:half]], axis=0), total
+    ).astype(BF)
 
 
 def per_device(
@@ -283,8 +293,18 @@
     )
     gated, decay, key, value, picked = front(*operands)
     full = exchange(gated, "tp", tp_order)
-    swap = [(zh * tp + t, t * tp + zh) for zh in range(planes) for t in range(tp)]
-    crossed = lax.ppermute(full, ("zh", "tp"), swap)
+    depth = len(zl_order)
+
+    def index(zh, zl, t):
+        return (zh * depth + zl) * tp + t
+
+    swap = []
+    for zh in range(planes):
+        for t in range(tp):
+            turn = depth // 2 if (t - zh) % planes == planes // 2 else 0
+            for zl in range(depth):
+                swap.append((index(zh, zl, t), index(t, (zl + turn) % depth, zh)))
+    crossed = lax.ppermute(full, ("zh", "zl", "tp"), swap)
 
     states = pl.pallas_call(
         states_kernel,

time: 77.8 us -> 75.4 us (0.969)
  waiting for transfers between devices: 17 us -> 15.4 us
  Pallas kernels: 9.34 us -> 7.92 us
    all_to_all x1, starting transfers between devices: 3.47 us -> 5.01 us  [exchange(): lax.all_to_all(pieces, axes, 0, 0, tiled=True, axis_index_groups=[list(or...]
    pallas_call x1, Pallas kernels: 5.37 us -> 3.97 us  [per_device(): gated, decay, key, value, picked = front(*operands)]
    ppermute x1, waiting for transfers between devices: 5.71 us -> 4.8 us  [per_device(): crossed = lax.ppermute(full, ('zh', 'zl', 'tp'), swap)]
    ppermute x1, starting transfers between devices: 20.8 us -> 19.9 us  [per_device(): crossed = lax.ppermute(full, ('zh', 'zl', 'tp'), swap)]
where the time goes in v3:
time: 75.4 us; the launch traced here: 75 us
  blocking collectives  26.1 us (35%)
  starting transfers between devices  24.9 us (33%)
  waiting for transfers between devices  15.4 us (20%)
  Pallas kernels  7.92 us (11%)
    all_to_all x2, blocking collectives, exchange(): lax.all_to_all(pieces, axes, 0, 0, tiled=True, axis_index_groups=[list(or...  26.1 us
    ppermute x1, starting transfers between devices, per_device(): crossed = lax.ppermute(full, ('zh', 'zl', 'tp'), swap)  19.9 us
    all_to_all x1, waiting for transfers between devices, exchange(): lax.all_to_all(pieces, axes, 0, 0, tiled=True, axis_index_groups=[list(or...  10.6 us
    all_to_all x1, starting transfers between devices, exchange(): lax.all_to_all(pieces, axes, 0, 0, tiled=True, axis_index_groups=[list(or...  5.01 us
    ppermute x1, waiting for transfers between devices, per_device(): crossed = lax.ppermute(full, ('zh', 'zl', 'tp'), swap)  4.8 us
    pallas_call x1, Pallas kernels, per_device(): gated, decay, key, value, picked = front(*operands)  3.97 us
  transfers between devices with their start and end apart: 2, of which 2 were waited for; matrix products, arithmetic and copies ran while one was open for 0% of the time, Pallas kernels for 2%

profile of v3, /device:TPU:4, one launch (start us, length us, event | category | flops | bytes accessed | tf_op | source)
XLA Modules:
  0.0 75.0 jit_solution(5714490224779453002)
XLA Ops:
  0.6 0.8 %shard_map.113 = bf16[8,24,512]{2,1,0:T(8,128)(2,1)S(1)} custom-call(bf16[2,4,512]{2,1,0:T(4,128)(2,1)} %rows_ref.1, bf16[32,256]{1,0:T(8,128)(2,1)} %bitcast.7), custom_call_target="tpu_custom_call" | custom-call | tf_op jit(solution)/shard_map/pallas_call | solution.py:250
  1.4 18.2 %all_to_all.15.refs_2_.refs_1_ = bf16[8,24,512]{2,1,0:T(8,128)(2,1)S(1)} all-to-all(bf16[8,24,512]{2,1,0:T(8,128)(2,1)S(1)} %shard_map.113), channel_id=1, replica_groups={{1,0,2,3,4,5,6,7},{9,8,10,11,12,13,14,15},{17,16,18,19,20,21,22,23},{25..., dimensions={0} | all-to-all | bytes 393216 | tf_op jit(solution)/shard_map/all_to_all | solution.py:21
  19.6 4.0 %shard_map.114 = (bf16[8,8,256]{2,1,0:T(8,128)(2,1)S(1)}, f32[8,256]{1,0:T(8,128)S(1)}, f32[8,256]{1,0:T(8,128)S(1)}, f32[8,256]{1,0:T(8,128)S(1)}, f32[2,256,128]{2,1,0:T(8,128)S(1)}) custom-call(s32[2]{0:T(128)} %refs_0_.1, f32[2,2,4]{2,1,0:T(2,128)} %bitcast.8, bf16[8,24,512]{2,1,0:T(8,128)(2,1)S(1)} %all_to_all.15.refs_2_.refs_1_, f32[1,4096]{1,0:T(1,128)} %bitcast.6, ...), custom_call_target="tpu_custom_call" | custom-call | flops 8388608 | bytes 6291456 | tf_op jit(solution)/shard_map/pallas_call | solution.py:294
  23.6 7.8 %all_to_all.16 = bf16[8,8,256]{2,1,0:T(8,128)(2,1)S(1)} all-to-all(bf16[8,8,256]{2,1,0:T(8,128)(2,1)S(1)} %get-tuple-element.7), channel_id=1, replica_groups={{1,0,2,3,4,5,6,7},{9,8,10,11,12,13,14,15},{17,16,18,19,20,21,22,23},{25..., dimensions={0} | all-to-all | bytes 65536 | tf_op jit(solution)/shard_map/all_to_all | solution.py:21
  31.5 19.9 %collective-permute-start = (bf16[8,8,256]{2,1,0:T(8,128)(2,1)S(1)}, bf16[8,8,256]{2,1,0:T(8,128)(2,1)S(1)}, u32[]{:S(2)}, u32[]{:S(2)}) collective-permute-start(bf16[8,8,256]{2,1,0:T(8,128)(2,1)S(1)} %all_to_all.16), channel_id=1, source_target_pairs={{0,0},{32,32},{64,64},{96,96},{1,128},{33,160},{65,192},{97,224},{... | collective-permute-start | bytes 98312 | tf_op jit(solution)/shard_map/ppermute | solution.py:307
  51.4 4.8 %collective-permute-done.rows_ref = bf16[8,8,256]{2,1,0:T(8,128)(2,1)S(1)} collective-permute-done((bf16[8,8,256]{2,1,0:T(8,128)(2,1)S(1)}, bf16[8,8,256]{2,1,0:T(8,128)(2,1)S(1)}, u32[]{:S(2)}, u32[]{:S(2)}) %collective-permute-start) | collective-permute-done | bytes 32800 | tf_op jit(solution)/shard_map/ppermute | solution.py:307
  56.2 0.8 %shard_map.115 = bf16[16,8,8,256]{3,2,1,0:T(8,128)(2,1)} custom-call(bf16[8,8,256]{2,1,0:T(8,128)(2,1)S(1)} %collective-permute-done.rows_ref), custom_call_target="tpu_custom_call" | custom-call | tf_op jit(solution)/shard_map/pallas_call | solution.py:319
  57.0 5.0 %all-to-all-start.2 = ((bf16[16,8,8,256]{3,2,1,0:T(8,128)(2,1)}), bf16[16,8,8,256]{3,2,1,0:T(8,128)(2,1)S(1)}, u32[]{:S(2)}, u32[]{:S(2)}) async-start(bf16[16,8,8,256]{3,2,1,0:T(8,128)(2,1)} %shard_map.115), calls=%async_computation.2 | async-start | bytes 1048576 | tf_op jit(solution)/shard_map/all_to_all | solution.py:21
  62.0 1.5 %shard_map.117 = f32[2,4,256,128]{3,2,1,0:T(8,128)} custom-call(f32[2,256,128]{2,1,0:T(8,128)S(1)} %get-tuple-element.8.picked_ref, f32[8,256]{1,0:T(8,128)S(1)} %get-tuple-element.9.decay_ref, f32[8,256]{1,0:T(8,128)S(1)} %get-tuple-element.10.key_ref, f32[8,256]{1,0:T(8,128)S(1)} %get-tuple-element.11.value_ref), custom_call_target="tpu_custom_call" | custom-call | flops 8388608 | bytes 1048576 | tf_op jit(solution)/shard_map/pallas_call | solution.py:317
  63.5 10.6 %all-to-all-done.2.refs_0_ = bf16[16,8,8,256]{3,2,1,0:T(8,128)(2,1)S(1)} async-done(((bf16[16,8,8,256]{3,2,1,0:T(8,128)(2,1)}), bf16[16,8,8,256]{3,2,1,0:T(8,128)(2,1)S(1)}, u32[]{:S(2)}, u32[]{:S(2)}) %all-to-all-start.2) | async-done | bytes 524320 | tf_op jit(solution)/shard_map/all_to_all | solution.py:21
  74.1 0.9 %shard_map.116 = bf16[128,32]{1,0:T(8,128)(2,1)} custom-call(bf16[16,8,8,256]{3,2,1,0:T(8,128)(2,1)S(1)} %all-to-all-done.2.refs_0_, bf16[8,24,512]{2,1,0:T(8,128)(2,1)S(1)} %all_to_all.15.refs_2_.refs_1_), custom_call_target="tpu_custom_call" | custom-call | tf_op jit(solution)/shard_map/pallas_call | solution.py:327
Async XLA Ops:
  31.5 24.7 %collective-permute-start = (bf16[8,8,256]{2,1,0:T(8,128)(2,1)S(1)}, bf16[8,8,256]{2,1,0:T(8,128)(2,1)S(1)}, u32[]{:S(2)}, u32[]{:S(2)}) collective-permute-start(bf16[8,8,256]{2,1,0:T(8,128)(2,1)S(1)} %all_to_all.16), channel_id=1, source_target_pairs={{0,0},{32,32},{64,64},{96,96},{1,128},{33,160},{65,192},{97,224},{... | collective-permute-start | bytes 98312 | tf_op jit(solution)/shard_map/ppermute | solution.py:307
  57.0 17.1 %all-to-all-start.2 = ((bf16[16,8,8,256]{3,2,1,0:T(8,128)(2,1)}), bf16[16,8,8,256]{3,2,1,0:T(8,128)(2,1)S(1)}, u32[]{:S(2)}, u32[]{:S(2)}) async-start(bf16[16,8,8,256]{3,2,1,0:T(8,128)(2,1)} %shard_map.115), calls=%async_computation.2 | async-start | bytes 1048576 | tf_op jit(solution)/shard_map/all_to_all | solution.py:21

commit v4 on v3

--- a/solution.py
+++ b/solution.py
@@ -12,7 +12,8 @@
 F32 = jnp.float32
 VM = pl.BlockSpec(memory_space=pltpu.VMEM)
 ZL_FIRST = 1
-TP_FIRST = 1
+Y_FIRST = 0
+TP_FIRST = 5
 AHEAD = 5
 HBM = pl.BlockSpec(memory_space=pltpu.HBM)
 
@@ -243,9 +244,8 @@
     slab = lax.axis_size(SLAB)
     shape = jax.ShapeDtypeStruct
     tp_order = led_by(tp, TP_FIRST)
-    zl_order = led_by(lax.axis_size("zl"), ZL_FIRST)
-    side = lax.axis_size("y")
-    slab_order = [zl * side + y for zl in zl_order for y in range(side)]
+    depth = lax.axis_size("zl")
+    slab_order = led_by(slab, ZL_FIRST * lax.axis_size("y") + Y_FIRST)
 
     pieces = pl.pallas_call(
         spread_kernel,
@@ -293,8 +293,6 @@
     )
     gated, decay, key, value, picked = front(*operands)
     full = exchange(gated, "tp", tp_order)
-    depth = len(zl_order)
-
     def index(zh, zl, t):
         return (zh * depth + zl) * tp + t
 

time: 75.4 us -> 74.1 us (0.983)
  starting transfers between devices: 24.9 us -> 19.8 us
  waiting for transfers between devices: 15.4 us -> 17.4 us
  blocking collectives: 26.1 us -> 27.8 us
    ppermute x1, waiting for transfers between devices: 4.8 us -> 8.38 us  [per_device(): crossed = lax.ppermute(full, ('zh', 'zl', 'tp'), swap)]
    ppermute x1, starting transfers between devices: 19.9 us -> 16.3 us  [per_device(): crossed = lax.ppermute(full, ('zh', 'zl', 'tp'), swap)]
    all_to_all x2, blocking collectives: 26.1 us -> 27.8 us  [exchange(): lax.all_to_all(pieces, axes, 0, 0, tiled=True, axis_index_groups=[list(or...]
    all_to_all x1, starting transfers between devices: 5.01 us -> 3.47 us  [exchange(): lax.all_to_all(pieces, axes, 0, 0, tiled=True, axis_index_groups=[list(or...]
    all_to_all x1, waiting for transfers between devices: 10.6 us -> 9.07 us  [exchange(): lax.all_to_all(pieces, axes, 0, 0, tiled=True, axis_index_groups=[list(or...]
where the time goes in v4:
time: 74.1 us; the launch traced here: 73.7 us
  blocking collectives  27.8 us (38%)
  starting transfers between devices  19.8 us (27%)
  waiting for transfers between devices  17.4 us (23%)
  Pallas kernels  7.95 us (11%)
    all_to_all x2, blocking collectives, exchange(): lax.all_to_all(pieces, axes, 0, 0, tiled=True, axis_index_groups=[list(or...  27.8 us
    ppermute x1, starting transfers between devices, per_device(): crossed = lax.ppermute(full, ('zh', 'zl', 'tp'), swap)  16.3 us
    all_to_all x1, waiting for transfers between devices, exchange(): lax.all_to_all(pieces, axes, 0, 0, tiled=True, axis_index_groups=[list(or...  9.07 us
    ppermute x1, waiting for transfers between devices, per_device(): crossed = lax.ppermute(full, ('zh', 'zl', 'tp'), swap)  8.38 us
    pallas_call x1, Pallas kernels, per_device(): gated, decay, key, value, picked = front(*operands)  3.99 us
    all_to_all x1, starting transfers between devices, exchange(): lax.all_to_all(pieces, axes, 0, 0, tiled=True, axis_index_groups=[list(or...  3.47 us
  transfers between devices with their start and end apart: 2, of which 2 were waited for; matrix products, arithmetic and copies ran while one was open for 0% of the time, Pallas kernels for 2%

profile of v4, /device:TPU:4, one launch (start us, length us, event | category | flops | bytes accessed | tf_op | source)
XLA Modules:
  0.0 73.7 jit_solution(7315298934627358228)
XLA Ops:
  0.6 0.8 %shard_map.113 = bf16[8,24,512]{2,1,0:T(8,128)(2,1)S(1)} custom-call(bf16[2,4,512]{2,1,0:T(4,128)(2,1)} %rows_ref.1, bf16[32,256]{1,0:T(8,128)(2,1)} %bitcast.7), custom_call_target="tpu_custom_call" | custom-call | tf_op jit(solution)/shard_map/pallas_call | solution.py:250
  1.4 20.7 %all_to_all.15.refs_2_.refs_1_ = bf16[8,24,512]{2,1,0:T(8,128)(2,1)S(1)} all-to-all(bf16[8,24,512]{2,1,0:T(8,128)(2,1)S(1)} %shard_map.113), channel_id=1, replica_groups={{5,0,1,2,3,4,6,7},{13,8,9,10,11,12,14,15},{21,16,17,18,19,20,22,23},{29..., dimensions={0} | all-to-all | bytes 393216 | tf_op jit(solution)/shard_map/all_to_all | solution.py:22
  22.1 4.0 %shard_map.114 = (bf16[8,8,256]{2,1,0:T(8,128)(2,1)S(1)}, f32[8,256]{1,0:T(8,128)S(1)}, f32[8,256]{1,0:T(8,128)S(1)}, f32[8,256]{1,0:T(8,128)S(1)}, f32[2,256,128]{2,1,0:T(8,128)S(1)}) custom-call(s32[2]{0:T(128)} %refs_0_.1, f32[2,2,4]{2,1,0:T(2,128)} %bitcast.8, bf16[8,24,512]{2,1,0:T(8,128)(2,1)S(1)} %all_to_all.15.refs_2_.refs_1_, f32[1,4096]{1,0:T(1,128)} %bitcast.6, ...), custom_call_target="tpu_custom_call" | custom-call | flops 8388608 | bytes 6291456 | tf_op jit(solution)/shard_map/pallas_call | solution.py:294
  26.1 7.1 %all_to_all.16 = bf16[8,8,256]{2,1,0:T(8,128)(2,1)S(1)} all-to-all(bf16[8,8,256]{2,1,0:T(8,128)(2,1)S(1)} %get-tuple-element.7), channel_id=1, replica_groups={{5,0,1,2,3,4,6,7},{13,8,9,10,11,12,14,15},{21,16,17,18,19,20,22,23},{29..., dimensions={0} | all-to-all | bytes 65536 | tf_op jit(solution)/shard_map/all_to_all | solution.py:22
  33.2 16.3 %collective-permute-start = (bf16[8,8,256]{2,1,0:T(8,128)(2,1)S(1)}, bf16[8,8,256]{2,1,0:T(8,128)(2,1)S(1)}, u32[]{:S(2)}, u32[]{:S(2)}) collective-permute-start(bf16[8,8,256]{2,1,0:T(8,128)(2,1)S(1)} %all_to_all.16), channel_id=1, source_target_pairs={{0,0},{32,32},{64,64},{96,96},{1,128},{33,160},{65,192},{97,224},{... | collective-permute-start | bytes 98312 | tf_op jit(solution)/shard_map/ppermute | solution.py:305
  49.6 8.4 %collective-permute-done.rows_ref = bf16[8,8,256]{2,1,0:T(8,128)(2,1)S(1)} collective-permute-done((bf16[8,8,256]{2,1,0:T(8,128)(2,1)S(1)}, bf16[8,8,256]{2,1,0:T(8,128)(2,1)S(1)}, u32[]{:S(2)}, u32[]{:S(2)}) %collective-permute-start) | collective-permute-done | bytes 32800 | tf_op jit(solution)/shard_map/ppermute | solution.py:305
  57.9 0.8 %shard_map.115 = bf16[16,8,8,256]{3,2,1,0:T(8,128)(2,1)} custom-call(bf16[8,8,256]{2,1,0:T(8,128)(2,1)S(1)} %collective-permute-done.rows_ref), custom_call_target="tpu_custom_call" | custom-call | tf_op jit(solution)/shard_map/pallas_call | solution.py:317
  58.8 3.5 %all-to-all-start.2 = ((bf16[16,8,8,256]{3,2,1,0:T(8,128)(2,1)}), bf16[16,8,8,256]{3,2,1,0:T(8,128)(2,1)S(1)}, u32[]{:S(2)}, u32[]{:S(2)}) async-start(bf16[16,8,8,256]{3,2,1,0:T(8,128)(2,1)} %shard_map.115), calls=%async_computation.2 | async-start | bytes 1048576 | tf_op jit(solution)/shard_map/all_to_all | solution.py:22
  62.2 1.5 %shard_map.117 = f32[2,4,256,128]{3,2,1,0:T(8,128)} custom-call(f32[2,256,128]{2,1,0:T(8,128)S(1)} %get-tuple-element.8.picked_ref, f32[8,256]{1,0:T(8,128)S(1)} %get-tuple-element.9.decay_ref, f32[8,256]{1,0:T(8,128)S(1)} %get-tuple-element.10.key_ref, f32[8,256]{1,0:T(8,128)S(1)} %get-tuple-element.11.value_ref), custom_call_target="tpu_custom_call" | custom-call | flops 8388608 | bytes 1048576 | tf_op jit(solution)/shard_map/pallas_call | solution.py:315
  63.7 9.1 %all-to-all-done.2.refs_0_ = bf16[16,8,8,256]{3,2,1,0:T(8,128)(2,1)S(1)} async-done(((bf16[16,8,8,256]{3,2,1,0:T(8,128)(2,1)}), bf16[16,8,8,256]{3,2,1,0:T(8,128)(2,1)S(1)}, u32[]{:S(2)}, u32[]{:S(2)}) %all-to-all-start.2) | async-done | bytes 524320 | tf_op jit(solution)/shard_map/all_to_all | solution.py:22
  72.8 0.9 %shard_map.116 = bf16[128,32]{1,0:T(8,128)(2,1)} custom-call(bf16[16,8,8,256]{3,2,1,0:T(8,128)(2,1)S(1)} %all-to-all-done.2.refs_0_, bf16[8,24,512]{2,1,0:T(8,128)(2,1)S(1)} %all_to_all.15.refs_2_.refs_1_), custom_call_target="tpu_custom_call" | custom-call | tf_op jit(solution)/shard_map/pallas_call | solution.py:325
Async XLA Ops:
  33.2 24.7 %collective-permute-start = (bf16[8,8,256]{2,1,0:T(8,128)(2,1)S(1)}, bf16[8,8,256]{2,1,0:T(8,128)(2,1)S(1)}, u32[]{:S(2)}, u32[]{:S(2)}) collective-permute-start(bf16[8,8,256]{2,1,0:T(8,128)(2,1)S(1)} %all_to_all.16), channel_id=1, source_target_pairs={{0,0},{32,32},{64,64},{96,96},{1,128},{33,160},{65,192},{97,224},{... | collective-permute-start | bytes 98312 | tf_op jit(solution)/shard_map/ppermute | solution.py:305
  58.8 14.0 %all-to-all-start.2 = ((bf16[16,8,8,256]{3,2,1,0:T(8,128)(2,1)}), bf16[16,8,8,256]{3,2,1,0:T(8,128)(2,1)S(1)}, u32[]{:S(2)}, u32[]{:S(2)}) async-start(bf16[16,8,8,256]{3,2,1,0:T(8,128)(2,1)} %shard_map.115), calls=%async_computation.2 | async-start | bytes 1048576 | tf_op jit(solution)/shard_map/all_to_all | solution.py:22

commit v5 on v4

--- a/solution.py
+++ b/solution.py
@@ -11,15 +11,29 @@
 BF = jnp.bfloat16
 F32 = jnp.float32
 VM = pl.BlockSpec(memory_space=pltpu.VMEM)
-ZL_FIRST = 1
-Y_FIRST = 0
+ZL_FIRST = 2
+Y_FIRST = 3
 TP_FIRST = 5
 AHEAD = 5
+HALF_TURN = (2, 3, 0, 1)
+NEAREST = (3, 2, 0, 1)
 HBM = pl.BlockSpec(memory_space=pltpu.HBM)
 
 
-def exchange(pieces, axes, order):
-    return lax.all_to_all(pieces, axes, 0, 0, tiled=True, axis_index_groups=[list(order)])
+def exchange(pieces, axes, *orders):
+    return lax.all_to_all(
+        pieces, axes, 0, 0, tiled=True, axis_index_groups=[list(order) for order in orders]
+    )
+
+
+def first_row():
+    at = [lax.axis_index(axis) for axis in KV]
+    return at[0] + at[1] + at[2] == 0
+
+
+def leads_turned(order):
+    first = first_row()
+    return [jnp.where(first, order[1], order[0]), jnp.where(first, order[0], order[1]), *order[2:]]
 
 
 def led_by(count, first):
@@ -83,10 +97,11 @@
     heads = channels // dim
     props = rows // seqs
     weights = (wq_ref, wf_ref, wv_ref)
+    spans = [pl.ds(pl.multiple_of(at * width, width), width) for at in leads_turned(order)]
     copies = [
         [
             pltpu.make_async_copy(
-                weight.at[pl.ds(order[block] * width, width)], held_ref.at[at, block], sems.at[at, block]
+                weight.at[spans[block]], held_ref.at[at, block], sems.at[at, block]
             )
             for at, weight in enumerate(weights)
         ]
@@ -111,7 +126,7 @@
     for block in range(blocks):
         x = x_ref[block, :rows].astype(F32)
         square = square + x * x
-        scaled.append((x * gain_ref[:, order[block] * width : (order[block] + 1) * width]).astype(BF))
+        scaled.append((x * gain_ref[:, spans[block]]).astype(BF))
     head_of = lax.broadcasted_iota(jnp.int32, (rows, channels), 1) // dim
     row_of = lax.broadcasted_iota(jnp.int32, (rows, channels), 0)
     extra = jnp.zeros((rows, channels), F32)
@@ -199,27 +214,53 @@
                 out_ref[seq, prop, span, :] = state
 
 
+def plane_for(zh, to, zl, y, planes):
+    if (to - zh) % planes != planes // 2:
+        return zl
+    table = NEAREST if y == 0 else HALF_TURN
+    return table[zl] if zh < to else table.index(zl)
+
+
+def is_far():
+    planes = lax.axis_size("zh")
+    return (lax.axis_index("tp") + planes - lax.axis_index("zh")) % planes == planes // 2
+
+
 def repeat_kernel(rows_ref, out_ref):
+    source = jnp.where(is_far(), NEAREST[0], 0)
+    turned = (lax.axis_index("tp") + lax.axis_index("y") == 0) & (lax.axis_index("zl") == source)
+    first = jnp.where(turned, 1, 0)
     for copy in range(out_ref.shape[0]):
-        out_ref[copy] = rows_ref[...]
+        out_ref[copy, 0] = rows_ref[first]
+        out_ref[copy, 1] = rows_ref[1 - first]
+        out_ref[copy, 2:] = rows_ref[2:]
 
 
 def product_kernel(order, rows, features, rows_ref, weight_ref, out_ref):
     members, blocks, _, channels = rows_ref.shape
-    half = features // 2
     total = jnp.zeros((members * rows, features), F32)
+    sources = leads_turned(list(range(blocks)))
     for block in range(blocks):
         left = jnp.concatenate([rows_ref[order.index(at), block] for at in range(members)], axis=0)
         right = jnp.concatenate(
-            [weight_ref[block, rows:, :channels], weight_ref[block, rows:, channels:]], axis=0
+            [
+                weight_ref[sources[block], rows:, :channels],
+                weight_ref[sources[block], rows:, channels:],
+            ],
+            axis=0,
         )
         total = total + contract_last(left, right)
-    planes = lax.axis_size("zh")
-    far = (lax.axis_index("tp") + planes - lax.axis_index("zh")) % planes == planes // 2
-    half = members * rows // 2
-    out_ref[...] = jnp.where(
-        far, jnp.concatenate([total[half:], total[:half]], axis=0), total
-    ).astype(BF)
+    planes, depth, side = (lax.axis_size(axis) for axis in KV)
+
+    def placed(zh, to):
+        at = [
+            plane_for(zh, to, zl, y, planes) * side + y for zl in range(depth) for y in range(side)
+        ]
+        return jnp.concatenate([total[member * rows : (member + 1) * rows] for member in at], axis=0)
+
+    upper = lax.axis_index("zh") >= planes // 2
+    far = jnp.where(upper, placed(0, planes // 2), placed(planes // 2, 0))
+    out_ref[...] = jnp.where(is_far(), far, total).astype(BF)
 
 
 def per_device(
@@ -259,7 +300,12 @@
         ],
         compiler_params=grant(4),
     )(in_hbm(proposals), in_hbm(output_matrix.T))
-    whole = exchange(pieces, "tp", tp_order)
+    turned = [tp_order[1], tp_order[0], *tp_order[2:]]
+    row_orders = [
+        [row * tp + t for t in (turned if row == 0 else tp_order)]
+        for row in range(planes * slab)
+    ]
+    whole = exchange(pieces, (*KV, "tp"), *row_orders)
 
     blocks = tp
     front = pl.pallas_call(
@@ -292,17 +338,20 @@
         in_hbm(prior_proposal_states),
     )
     gated, decay, key, value, picked = front(*operands)
-    full = exchange(gated, "tp", tp_order)
-    def index(zh, zl, t):
-        return (zh * depth + zl) * tp + t
-
-    swap = []
-    for zh in range(planes):
-        for t in range(tp):
-            turn = depth // 2 if (t - zh) % planes == planes // 2 else 0
-            for zl in range(depth):
-                swap.append((index(zh, zl, t), index(t, (zl + turn) % depth, zh)))
-    crossed = lax.ppermute(full, ("zh", "zl", "tp"), swap)
+    full = exchange(gated, (*KV, "tp"), *row_orders)
+    side = lax.axis_size("y")
+
+    def index(zh, zl, y, t):
+        return ((zh * depth + zl) * side + y) * tp + t
+
+    swap = [
+        (index(zh, zl, y, t), index(t, plane_for(zh, t, zl, y, planes), y, zh))
+        for zh in range(planes)
+        for zl in range(depth)
+        for y in range(side)
+        for t in range(tp)
+    ]
+    crossed = lax.ppermute(full, (*KV, "tp"), swap)
 
     states = pl.pallas_call(
         states_kernel,

time: 74.1 us -> 73.9 us (level)
  starting transfers between devices: 19.8 us -> 23 us
  waiting for transfers between devices: 17.4 us -> 14.9 us
  blocking collectives: 27.8 us -> 27 us
    all_to_all x1, starting transfers between devices: 3.47 us -> 6.32 us  [exchange(): lax.all_to_all(pieces, axes, 0, 0, tiled=True, axis_index_groups=[list(or...]
    all_to_all x1, waiting for transfers between devices: 9.07 us -> 7.76 us  [exchange(): lax.all_to_all(pieces, axes, 0, 0, tiled=True, axis_index_groups=[list(or...]
    ppermute x1, waiting for transfers between devices: 8.38 us -> 7.11 us  [per_device(): crossed = lax.ppermute(full, (*KV, 'tp'), swap)]
    all_to_all x2, blocking collectives: 27.8 us -> 27 us  [exchange(): lax.all_to_all(pieces, axes, 0, 0, tiled=True, axis_index_groups=[list(or...]
where the time goes in v5:
time: 73.9 us; the launch traced here: 73.5 us
  blocking collectives  27 us (37%)
  starting transfers between devices  23 us (31%)
  waiting for transfers between devices  14.9 us (20%)
  Pallas kernels  7.97 us (11%)
    all_to_all x2, blocking collectives, exchange(): lax.all_to_all(pieces, axes, 0, 0, tiled=True, axis_index_groups=[list(or...  27 us
    ppermute x1, starting transfers between devices, per_device(): crossed = lax.ppermute(full, (*KV, 'tp'), swap)  16.7 us
    all_to_all x1, waiting for transfers between devices, exchange(): lax.all_to_all(pieces, axes, 0, 0, tiled=True, axis_index_groups=[list(or...  7.76 us
    ppermute x1, waiting for transfers between devices, per_device(): crossed = lax.ppermute(full, (*KV, 'tp'), swap)  7.11 us
    all_to_all x1, starting transfers between devices, exchange(): lax.all_to_all(pieces, axes, 0, 0, tiled=True, axis_index_groups=[list(or...  6.32 us
    pallas_call x1, Pallas kernels, per_device(): gated, decay, key, value, picked = front(*operands)  3.99 us
  transfers between devices with their start and end apart: 2, of which 2 were waited for; matrix products, arithmetic and copies ran while one was open for 0% of the time, Pallas kernels for 2%

profile of v5, /device:TPU:4, one launch (start us, length us, event | category | flops | bytes accessed | tf_op | source)
XLA Modules:
  0.0 73.5 jit_solution(4406935615375435629)
XLA Ops:
  0.6 0.8 %shard_map.113 = bf16[8,24,512]{2,1,0:T(8,128)(2,1)S(1)} custom-call(bf16[2,4,512]{2,1,0:T(4,128)(2,1)} %rows_ref.1, bf16[32,256]{1,0:T(8,128)(2,1)} %bitcast.7), custom_call_target="tpu_custom_call" | custom-call | tf_op jit(solution)/shard_map/pallas_call | solution.py:291
  1.4 19.2 %all_to_all.15.refs_2_.refs_1_ = bf16[8,24,512]{2,1,0:T(8,128)(2,1)S(1)} all-to-all(bf16[8,24,512]{2,1,0:T(8,128)(2,1)S(1)} %shard_map.113), channel_id=1, replica_groups={{0,5,1,2,3,4,6,7},{13,8,9,10,11,12,14,15},{21,16,17,18,19,20,22,23},{29..., dimensions={0} | all-to-all | bytes 393216 | tf_op jit(solution)/shard_map/all_to_all | solution.py:24
  20.6 4.0 %shard_map.114 = (bf16[8,8,256]{2,1,0:T(8,128)(2,1)S(1)}, f32[8,256]{1,0:T(8,128)S(1)}, f32[8,256]{1,0:T(8,128)S(1)}, f32[8,256]{1,0:T(8,128)S(1)}, f32[2,256,128]{2,1,0:T(8,128)S(1)}) custom-call(s32[2]{0:T(128)} %refs_0_.1, f32[2,2,4]{2,1,0:T(2,128)} %bitcast.8, bf16[8,24,512]{2,1,0:T(8,128)(2,1)S(1)} %all_to_all.15.refs_2_.refs_1_, f32[1,4096]{1,0:T(1,128)} %bitcast.6, ...), custom_call_target="tpu_custom_call" | custom-call | flops 8388608 | bytes 6291456 | tf_op jit(solution)/shard_map/pallas_call | solution.py:340
  24.6 7.8 %all_to_all.16 = bf16[8,8,256]{2,1,0:T(8,128)(2,1)S(1)} all-to-all(bf16[8,8,256]{2,1,0:T(8,128)(2,1)S(1)} %get-tuple-element.7), channel_id=1, replica_groups={{0,5,1,2,3,4,6,7},{13,8,9,10,11,12,14,15},{21,16,17,18,19,20,22,23},{29..., dimensions={0} | all-to-all | bytes 65536 | tf_op jit(solution)/shard_map/all_to_all | solution.py:24
  32.4 16.7 %collective-permute-start = (bf16[8,8,256]{2,1,0:T(8,128)(2,1)S(1)}, bf16[8,8,256]{2,1,0:T(8,128)(2,1)S(1)}, u32[]{:S(2)}, u32[]{:S(2)}) collective-permute-start(bf16[8,8,256]{2,1,0:T(8,128)(2,1)S(1)} %all_to_all.16), channel_id=1, source_target_pairs={{0,0},{1,128},{2,256},{3,384},{4,608},{5,640},{6,768},{7,896},{8,8... | collective-permute-start | bytes 98312 | tf_op jit(solution)/shard_map/ppermute | solution.py:354
  49.1 7.1 %collective-permute-done.rows_ref = bf16[8,8,256]{2,1,0:T(8,128)(2,1)S(1)} collective-permute-done((bf16[8,8,256]{2,1,0:T(8,128)(2,1)S(1)}, bf16[8,8,256]{2,1,0:T(8,128)(2,1)S(1)}, u32[]{:S(2)}, u32[]{:S(2)}) %collective-permute-start) | collective-permute-done | bytes 32800 | tf_op jit(solution)/shard_map/ppermute | solution.py:354
  56.2 0.8 %shard_map.115 = bf16[16,8,8,256]{3,2,1,0:T(8,128)(2,1)} custom-call(bf16[8,8,256]{2,1,0:T(8,128)(2,1)S(1)} %collective-permute-done.rows_ref), custom_call_target="tpu_custom_call" | custom-call | tf_op jit(solution)/shard_map/pallas_call | solution.py:366
  57.1 6.3 %all-to-all-start.2 = ((bf16[16,8,8,256]{3,2,1,0:T(8,128)(2,1)}), bf16[16,8,8,256]{3,2,1,0:T(8,128)(2,1)S(1)}, u32[]{:S(2)}, u32[]{:S(2)}) async-start(bf16[16,8,8,256]{3,2,1,0:T(8,128)(2,1)} %shard_map.115), calls=%async_computation.2 | async-start | bytes 1048576 | tf_op jit(solution)/shard_map/all_to_all | solution.py:24
  63.4 1.5 %shard_map.117 = f32[2,4,256,128]{3,2,1,0:T(8,128)} custom-call(f32[2,256,128]{2,1,0:T(8,128)S(1)} %get-tuple-element.8.picked_ref, f32[8,256]{1,0:T(8,128)S(1)} %get-tuple-element.9.decay_ref, f32[8,256]{1,0:T(8,128)S(1)} %get-tuple-element.10.key_ref, f32[8,256]{1,0:T(8,128)S(1)} %get-tuple-element.11.value_ref), custom_call_target="tpu_custom_call" | custom-call | flops 8388608 | bytes 1048576 | tf_op jit(solution)/shard_map/pallas_call | solution.py:364
  64.9 7.8 %all-to-all-done.2.refs_0_ = bf16[16,8,8,256]{3,2,1,0:T(8,128)(2,1)S(1)} async-done(((bf16[16,8,8,256]{3,2,1,0:T(8,128)(2,1)}), bf16[16,8,8,256]{3,2,1,0:T(8,128)(2,1)S(1)}, u32[]{:S(2)}, u32[]{:S(2)}) %all-to-all-start.2) | async-done | bytes 524320 | tf_op jit(solution)/shard_map/all_to_all | solution.py:24
  72.6 0.9 %shard_map.116 = bf16[128,32]{1,0:T(8,128)(2,1)} custom-call(bf16[16,8,8,256]{3,2,1,0:T(8,128)(2,1)S(1)} %all-to-all-done.2.refs_0_, bf16[8,24,512]{2,1,0:T(8,128)(2,1)S(1)} %all_to_all.15.refs_2_.refs_1_), custom_call_target="tpu_custom_call" | custom-call | tf_op jit(solution)/shard_map/pallas_call | solution.py:374
Async XLA Ops:
  32.4 23.8 %collective-permute-start = (bf16[8,8,256]{2,1,0:T(8,128)(2,1)S(1)}, bf16[8,8,256]{2,1,0:T(8,128)(2,1)S(1)}, u32[]{:S(2)}, u32[]{:S(2)}) collective-permute-start(bf16[8,8,256]{2,1,0:T(8,128)(2,1)S(1)} %all_to_all.16), channel_id=1, source_target_pairs={{0,0},{1,128},{2,256},{3,384},{4,608},{5,640},{6,768},{7,896},{8,8... | collective-permute-start | bytes 98312 | tf_op jit(solution)/shard_map/ppermute | solution.py:354
  57.1 15.6 %all-to-all-start.2 = ((bf16[16,8,8,256]{3,2,1,0:T(8,128)(2,1)}), bf16[16,8,8,256]{3,2,1,0:T(8,128)(2,1)S(1)}, u32[]{:S(2)}, u32[]{:S(2)}) async-start(bf16[16,8,8,256]{3,2,1,0:T(8,128)(2,1)} %shard_map.115), calls=%async_computation.2 | async-start | bytes 1048576 | tf_op jit(solution)/shard_map/all_to_all | solution.py:24
